TPU v7x, 256 devices: a whole 4x4x8 slice. The times are simulated.
256 devices in a mesh: ep: 32 (over z, x), tp: 8 (over y, core).
Axes of the slice: x: 4, y: 4, z: 8, core: 2. Of those that a mesh axis runs over, the one named last changes fastest.
Arguments:
- stream: bfloat16 [8192, 3072], P('ep'), may hold values from -30 to 30
- ffn_gain: bfloat16 [3072], replicated, may hold values from 0.099609375 to 1.8984375
- chosen: int32 [32, 1024], replicated, may hold values from 0 to 8191, as said below
- affinity: float32 [32, 1024], P('ep'), may hold values from 0.5 to 2
- w_gate: bfloat16 [32, 3072, 3072], P('ep', None, 'tp'), may hold values from -0.109375 to 0.109375
- w_up: bfloat16 [32, 3072, 3072], P('ep', None, 'tp'), may hold values from -0.109375 to 0.109375
- w_down: bfloat16 [32, 3072, 3072], P('ep', 'tp'), may hold values from -0.109375 to 0.109375
- final_gain: bfloat16 [3072], P('tp'), may hold values from 0.099609375 to 1.8984375
Outputs:
- normed: bfloat16 [8192, 3072], P('ep', 'tp')
Inputs may be any that keep to these rules, and one draw needn't show every extreme that they name: `chosen`: row e holds 1024 distinct token numbers in ascending order. Of the 256 tokens of one index of ep, each expert reads at least one and at most 48; in every draw some expert reads exactly 48 from some index.
All inputs are finite; a program needn't handle non-finite values.
Results may differ from a plain program's by a relative error of at most 0.015.
Values may be sent and summed in bfloat16 or wider, within the bound.
A program may use at most 128 MiB of HBM per device.

v0:
```python
import jax
import jax.numpy as jnp
from jax import lax
from jax.sharding import PartitionSpec as P

EPSILON = 1e-06


def sent_to_all(array, axis):
    devices = lax.axis_size(axis)
    return lax.all_to_all(
        jnp.broadcast_to(array[None], (devices, *array.shape)), axis, 0, 0, tiled=True
    )


def over_copies(array, axis):
    return sent_to_all(array, axis).sum(axis=0)


def on_device(stream, ffn_gain, chosen, affinity, w_gate, w_up, w_down, final_gain):
    tok_rows = stream.shape[0]
    model_width = stream.shape[1]
    experts = chosen.shape[0]
    picks = chosen.shape[1]
    ep_count = lax.axis_size("ep")
    tp_count = lax.axis_size("tp")
    device = lax.axis_index("ep")
    column = lax.axis_index("tp")
    share_width = model_width // tp_count
    slots = 3 * tok_rows // 16
    widened = stream.astype(jnp.float32)
    scale_in = lax.rsqrt(jnp.mean(widened * widened, axis=-1, keepdims=True) + EPSILON)
    normed_in = (widened * scale_in * ffn_gain.astype(jnp.float32)).astype(jnp.bfloat16)
    source = chosen // tok_rows
    counts = jnp.sum(
        (source[:, :, None] == jnp.arange(ep_count)[None, None, :]).astype(jnp.int32), axis=1
    )
    starts = jnp.cumsum(counts, axis=1) - counts
    slot_range = jnp.arange(slots, dtype=jnp.int32)
    own_start = jnp.take(starts, device, axis=1)
    own_count = jnp.take(counts, device, axis=1)
    send_pos = jnp.clip(own_start[:, None] + slot_range[None, :], 0, picks - 1)
    send_valid = slot_range[None, :] < own_count[:, None]
    local_tok = jnp.where(
        send_valid, jnp.take_along_axis(chosen, send_pos, axis=1) - device * tok_rows, 0
    )
    local_flat = local_tok.reshape(-1)
    row_source = jnp.take(source, device, axis=0)
    row_starts = jnp.take(starts, device, axis=0)
    arrival = (
        row_source * slots + jnp.arange(picks, dtype=jnp.int32) - jnp.take(row_starts, row_source)
    )
    gate_rows = w_gate[0]
    up_rows = w_up[0]
    own_columns = lax.dynamic_slice_in_dim(normed_in, column * share_width, share_width, 1)
    outgoing = jnp.take(own_columns, local_flat, axis=0).reshape(experts, slots, share_width)
    arrived = lax.all_to_all(outgoing, "ep", split_axis=0, concat_axis=0, tiled=True)
    shared = jnp.take(arrived.reshape(-1, share_width), arrival, axis=0)
    piece = lax.all_gather(shared, "tp", axis=1, tiled=True)
    gate = jnp.dot(piece, gate_rows, preferred_element_type=jnp.float32)
    up = jnp.dot(piece, up_rows, preferred_element_type=jnp.float32)
    hidden = (jax.nn.silu(gate) * up).astype(jnp.bfloat16)
    down_rows = w_down[0]
    piece = down_rows
    expert_cols = lax.psum_scatter(
        lax.dot_general(
            piece, hidden, (((0,), (1,)), ((), ())), preferred_element_type=jnp.float32
        ).astype(jnp.bfloat16),
        "tp",
        scatter_dimension=0,
        tiled=True,
    ).astype(jnp.float32)
    weighted = (expert_cols * affinity[0][None, :]).astype(jnp.bfloat16)
    slot_pos = jnp.clip(row_starts[:, None] + slot_range[None, :], 0, picks - 1)
    leaving = jnp.take(weighted, slot_pos.reshape(-1), axis=1).reshape(share_width, ep_count, slots)
    returned = lax.all_to_all(leaving, "ep", split_axis=1, concat_axis=1, tiled=True)
    placing = (
        (local_flat[:, None] == jnp.arange(tok_rows, dtype=jnp.int32)[None, :])
        & send_valid.reshape(-1)[:, None]
    ).astype(jnp.bfloat16)
    update = lax.dot_general(
        placing,
        returned.reshape(share_width, -1),
        (((0,), (1,)), ((), ())),
        preferred_element_type=jnp.float32,
    )
    own_stream = lax.dynamic_slice_in_dim(widened, column * share_width, share_width, 1)
    merged = own_stream + update
    totals = over_copies(jnp.sum(merged * merged, axis=1), "tp")
    scale_out = lax.rsqrt(totals[:, None] / model_width + EPSILON)
    return (merged * scale_out * final_gain.astype(jnp.float32)[None, :]).astype(jnp.bfloat16)


def solution(mesh):
    return jax.shard_map(
        on_device,
        mesh=mesh,
        in_specs=(
            P("ep", None),
            P(),
            P(),
            P("ep", None),
            P("ep", None, "tp"),
            P("ep", None, "tp"),
            P("ep", "tp", None),
            P("tp"),
        ),
        out_specs=P("ep", "tp"),
        check_vma=False,
    )
```

profile of v0, /device:TPU:1, one launch (start us, length us, event | category | flops | bytes accessed | tf_op | source)
XLA Modules:
  0.0 273.2 jit_solution(4535225694800903247)
XLA Ops:
  6.5 2.0 multiply_reduce_fusion
  8.5 0.1 copy-done.2
  8.6 2.0 convert_element_type.34
  10.6 0.1 lt.201
  10.7 0.1 add_select_fusion
  10.8 0.0 copy-start.3
  10.8 0.6 copy-done.3
  11.5 0.6 convert_reduce_fusion
  12.1 0.2 reduce_window_sum.11
  12.3 0.2 select_reduce_fusion
  12.5 0.1 fusion.21
  12.6 0.1 add.254
  12.7 0.6 copy-done.4
  13.3 0.1 add.280
  13.3 0.1 reshape.527
  13.4 12.6 %gather_fusion.3 = s32[1536]{0:T(1024)S(1)} fusion(s32[32,1024]{1,0:T(8,128)S(1)} %copy-done.1, s32[1536]{0:T(1024)S(1)} %reshape.527), kind=kCustom, calls=%fused_computation.3 | custom fusion | bytes 24576 | tf_op jit(solution)/shard_map/jit(take_along_axis)/gather | solution.py:45
  26.0 0.1 reshape.530
  26.1 0.1 compare_and_fusion
  26.2 0.1 lt.199
  26.3 0.1 fusion.25
  26.4 0.8 dynamic-slice.15
  27.2 1.1 multiply_convert_fusion.3
  28.3 5.3 %gather_fusion = bf16[1536,384]{1,0:T(8,128)(2,1)} fusion(bf16[256,384]{1,0:T(8,128)(2,1)S(1)} %multiply_convert_fusion.3, s32[2048]{0:T(1024)S(1)} %pad_clamp_fusion.1), kind=kCustom, calls=%fused_computation | custom fusion | bytes 2365440 | tf_op jit(solution)/shard_map/jit(_take)/gather | solution.py:56
  33.6 2.6 broadcast_select_fusion
  36.1 11.9 %all-to-all-start = ((bf16[32,48,384]{2,1,0:T(8,128)(2,1)}), bf16[32,48,384]{2,1,0:T(8,128)(2,1)S(1)}, u32[]{:S(2)}, u32[]{:S(2)}) async-start(bf16[32,48,384]{2,1,0:T(8,128)(2,1)} %broadcast_select_fusion), calls=%async_computation | async-start | bytes 2359296 | tf_op jit(solution)/shard_map/all_to_all | solution.py:57
  48.0 0.0 all-gather.2.cloned.1.call-start
  48.0 0.7 broadcast_select_fusion.4
  48.7 0.7 fusion.30
  49.5 4.9 %compare_select_fusion.10 = (s32[1024,1]{0,1:T(1,128)S(1)}, s32[1024,1]{0,1:T(1,128)S(1)}, s32[1,1024]{1,0:T(1,128)S(1)}) fusion(s32[]{:T(128)} %bitcast.28, s32[]{:T(128)} %bitcast.29, s32[]{:T(128)} %bitcast.30, s32[]{:T(128)} %bitcast.31, s32[]{:T(128)} %bitcast.32, s32[]{:T(128)} %bitcast.34, s32[]{:T(128)} %bitcast.33, s32[32,1024]{1,0:T(8,128)} %copy-done.3, ...), kind=kLoop, calls=%fused_computation.80 | loop fusion | flops 16384 | bytes 16417 | tf_op jit(solution)/shard_map/jit(_take)/gather | solution.py:51
  54.4 0.7 fusion.31
  55.1 0.3 compare_reduce_fusion.24
  55.3 16.2 %compare_and_fusion.2 = (pred[1024]{0:T(1024)(128)(4,1)}, s32[1024]{0:T(1024)S(1)}) fusion(s32[1024]{0:T(1024)S(1)} %bitcast.88, pred[1024]{0:T(1024)(128)(4,1)S(1)} %get-tuple-element.63, pred[1024]{0:T(1024)(128)(4,1)S(1)} %get-tuple-element.61, pred[1024]{0:T(1024)(128)(4,1)S(1)} %get-tuple-element.62, pred[1024]{0:T(1024)(128)(4,1)S(1)} %get-tuple-element.60, ...), kind=kLoop, calls=%fused_computation.101 | loop fusion | flops 41984 | bytes 39012 | tf_op jit(solution)/shard_map/jit(_take)/and | solution.py:58
  71.6 5.1 %all-to-all-done = bf16[32,48,384]{2,1,0:T(8,128)(2,1)S(1)} async-done(((bf16[32,48,384]{2,1,0:T(8,128)(2,1)}), bf16[32,48,384]{2,1,0:T(8,128)(2,1)S(1)}, u32[]{:S(2)}, u32[]{:S(2)}) %all-to-all-start) | async-done | bytes 1179680 | tf_op jit(solution)/shard_map/all_to_all | solution.py:57
  76.7 5.0 %gather_fusion.1 = bf16[1024,384]{1,0:T(8,128)(2,1)} fusion(bf16[1536,384]{1,0:T(8,128)(2,1)S(1)} %bitcast.84, s32[1024]{0:T(1024)S(1)} %broadcast_clamp_fusion), kind=kCustom, calls=%fused_computation.1 | custom fusion | bytes 1576960 | tf_op jit(solution)/shard_map/jit(_take)/gather | solution.py:58
  81.6 2.2 broadcast_select_fusion.2
  83.9 0.0 all-gather.2.cloned.1.call-update
  83.9 0.0 reduce-scatter.4.cloned.1.call-start
  83.9 43.6 %all-gather.2.cloned.1.call-done = bf16[1024,3072]{1,0:T(8,128)(2,1)} async-done(((bf16[1024,384]{1,0:T(8,128)(2,1)}), bf16[1024,3072]{1,0:T(8,128)(2,1)}) %all-gather.2.cloned.1.call-update) | async-done | bytes 6291472 | tf_op jit(solution)/shard_map/all_gather | solution.py:59
  127.5 8.0 %fusion.3 = f32[1024,384]{1,0:T(8,128)} fusion(bf16[1024,3072]{1,0:T(8,128)(2,1)} %all-gather.2.cloned.1.call-done, bf16[1,3072,384]{2,1,0:T(8,128)(2,1)} %param.14), kind=kOutput, calls=%fused_computation.11 | convolution fusion | flops 2415919104 | bytes 10223616 | tf_op jit(solution)/shard_map/dot_general | solution.py:60
  135.5 11.4 %convert_bitcast_fusion = bf16[3072,1024]{0,1:T(8,128)(2,1)} fusion(bf16[1,384,3072]{2,1,0:T(8,128)(2,1)S(1)} %copy-done, f32[1024,384]{1,0:T(8,128)} %fusion.3, bf16[1024,3072]{1,0:T(8,128)(2,1)} %all-gather.2.cloned.1.call-done, bf16[1,3072,384]{2,1,0:T(8,128)(2,1)} %param.15), kind=kOutput, calls=%fused_computation.4 | convolution fusion | flops 4837343232 | bytes 18874368 | tf_op jit(solution)/shard_map/dot_general | solution.py:66
  146.9 8.7 %copy.10 = bf16[3072,1024]{1,0:T(8,128)(2,1)} copy(bf16[3072,1024]{0,1:T(8,128)(2,1)} %convert_bitcast_fusion) | data formatting | bytes 12582912
  155.6 0.0 reduce-scatter.4.cloned.1.call-update
  155.6 0.0 copy-start.6
  155.6 0.7 fusion.35
  156.3 0.1 add_clamp_fusion
  156.4 0.1 min.35
  156.5 0.1 compare_and_fusion.1
  156.6 43.4 %reduce-scatter.4.cloned.1.call-done = bf16[384,1024]{1,0:T(8,128)(2,1)} async-done(((bf16[3072,1024]{1,0:T(8,128)(2,1)}), bf16[384,1024]{1,0:T(8,128)(2,1)}) %reduce-scatter.4.cloned.1.call-update) | async-done | bytes 786448
  200.0 2.3 copy.11
  202.3 1.3 multiply_convert_fusion
  203.6 5.3 %gather_fusion.2 = bf16[1536,384]{1,0:T(8,128)(2,1)} fusion(bf16[384,1024]{0,1:T(8,128)(2,1)S(1)} %multiply_convert_fusion, s32[2048]{0:T(1024)S(1)} %pad_clamp_fusion), kind=kCustom, calls=%fused_computation.2 | custom fusion | bytes 2365440 | tf_op jit(solution)/shard_map/jit(_take)/gather | solution.py:75
  208.9 2.6 broadcast_select_fusion.1
  211.5 9.5 %all-to-all-start.1 = ((bf16[384,32,48]{0,2,1:T(8,128)(2,1)}), bf16[384,32,48]{0,2,1:T(8,128)(2,1)S(1)}, u32[]{:S(2)}, u32[]{:S(2)}) async-start(bf16[384,32,48]{0,2,1:T(8,128)(2,1)} %broadcast_select_fusion.1), calls=%async_computation.1 | async-start | bytes 2359296 | tf_op jit(solution)/shard_map/all_to_all | solution.py:76
  221.0 1.4 add.255
  222.4 0.7 lt.182
  223.1 0.6 lt.183
  223.7 0.8 lt.184
  224.5 1.3 subtract_select_fusion
  225.8 23.7 %all-to-all-done.1 = bf16[384,32,48]{0,2,1:T(8,128)(2,1)S(1)} async-done(((bf16[384,32,48]{0,2,1:T(8,128)(2,1)}), bf16[384,32,48]{0,2,1:T(8,128)(2,1)S(1)}, u32[]{:S(2)}, u32[]{:S(2)}) %all-to-all-start.1) | async-done | bytes 1179680 | tf_op jit(solution)/shard_map/all_to_all | solution.py:76
  249.5 2.9 %multiply_reduce_fusion.1 = (f32[256]{0:T(256)S(1)}, f32[256,384]{1,0:T(8,128)}) fusion(bf16[384,1536]{0,1:T(8,128)(2,1)S(1)} %bitcast.87, s32[1536]{0:T(1024)} %subtract_select_fusion, pred[1536]{0:T(1024)(128)(4,1)} %lt.182, f32[256,3072]{1,0:T(8,128)} %convert_element_type.34, s32[]{:T(128)S(6)} %select_n.231), kind=kOutput, calls=%fused_computation.25 | convolution fusion | flops 303070976 | bytes 1974788 | tf_op jit(solution)/shard_map/dot_general | solution.py:81
  252.4 0.6 broadcast_in_dim.111
  253.0 7.0 %all-to-all-start.2 = ((f32[8,1,256]{2,1,0:T(1,128)}), f32[8,1,256]{2,1,0:T(1,128)S(1)}, u32[]{:S(2)}, u32[]{:S(2)}) async-start(f32[8,1,256]{2,1,0:T(1,128)} %broadcast_in_dim.111), calls=%async_computation.2 | async-start | bytes 16384 | tf_op jit(solution)/shard_map/all_to_all | solution.py:11
  260.0 4.6 %all-to-all-done.2 = f32[8,1,256]{2,1,0:T(1,128)S(1)} async-done(((f32[8,1,256]{2,1,0:T(1,128)}), f32[8,1,256]{2,1,0:T(1,128)S(1)}, u32[]{:S(2)}, u32[]{:S(2)}) %all-to-all-start.2) | async-done | bytes 8224 | tf_op jit(solution)/shard_map/all_to_all | solution.py:11
  264.6 1.8 multiply_convert_fusion.2
  (22 shorter events, 0.1 us)
Async XLA Ops:
  6.5 129.0 %copy-start = (bf16[1,384,3072]{2,1,0:T(8,128)(2,1)S(1)}, bf16[1,384,3072]{2,1,0:T(8,128)(2,1)}, u32[]{:S(2)}) copy-start(bf16[1,384,3072]{2,1,0:T(8,128)(2,1)} %param.16) | copy-start | bytes 7077892
  6.5 2.0 copy-start.2
  8.6 2.1 copy-start.1
  10.8 0.7 copy-start.3
  12.3 13.7 %copy-start.5 = (s32[32,32]{1,0:T(8,128)}, s32[32,32]{1,0:T(8,128)S(1)}, u32[]{:S(2)}) copy-start(s32[32,32]{1,0:T(8,128)S(1)} %sub.52) | copy-start | bytes 12292
  12.7 0.6 copy-start.4
  36.1 40.5 %all-to-all-start = ((bf16[32,48,384]{2,1,0:T(8,128)(2,1)}), bf16[32,48,384]{2,1,0:T(8,128)(2,1)S(1)}, u32[]{:S(2)}, u32[]{:S(2)}) async-start(bf16[32,48,384]{2,1,0:T(8,128)(2,1)} %broadcast_select_fusion), calls=%async_computation | async-start | bytes 2359296 | tf_op jit(solution)/shard_map/all_to_all | solution.py:57
  48.0 79.5 %all-gather.2.cloned.1.call-start = ((), (), s32[]{:S(2)}) async-start(), calls=%async_computation.4 | async-start | bytes 7077888 | tf_op jit(solution)/shard_map/all_gather | solution.py:59
  83.9 116.1 %reduce-scatter.4.cloned.1.call-start = ((), (), s32[]{:S(2)}) async-start(), calls=%async_computation.5 | async-start | bytes 7077888
  155.6 46.7 %copy-start.6 = (f32[1,1024]{1,0:T(1,128)S(1)}, f32[1,1024]{1,0:T(1,128)}, u32[]{:S(2)}) copy-start(f32[1,1024]{1,0:T(1,128)} %param.13) | copy-start | bytes 12292
  211.5 38.0 %all-to-all-start.1 = ((bf16[384,32,48]{0,2,1:T(8,128)(2,1)}), bf16[384,32,48]{0,2,1:T(8,128)(2,1)S(1)}, u32[]{:S(2)}, u32[]{:S(2)}) async-start(bf16[384,32,48]{0,2,1:T(8,128)(2,1)} %broadcast_select_fusion.1), calls=%async_computation.1 | async-start | bytes 2359296 | tf_op jit(solution)/shard_map/all_to_all | solution.py:76
  225.8 34.2 %copy-start.7 = (bf16[384]{0:T(512)(128)(2,1)S(1)}, bf16[384]{0:T(512)(128)(2,1)}, u32[]{:S(2)}) copy-start(bf16[384]{0:T(512)(128)(2,1)} %param.17) | copy-start | bytes 2308
  253.0 11.6 %all-to-all-start.2 = ((f32[8,1,256]{2,1,0:T(1,128)}), f32[8,1,256]{2,1,0:T(1,128)S(1)}, u32[]{:S(2)}, u32[]{:S(2)}) async-start(f32[8,1,256]{2,1,0:T(1,128)} %broadcast_in_dim.111), calls=%async_computation.2 | async-start | bytes 16384 | tf_op jit(solution)/shard_map/all_to_all | solution.py:11
Sparse Core Ops, SparseCore 0:
  84.0 43.4 all-gather.1
  155.7 44.2 reduce-scatter.3
where the time goes:
time: 275 us; the launch traced here: 273 us
  waiting for transfers between devices  120 us (44%)
  local copies, waits for them, and re-layouts  47.3 us (17%)
  other arithmetic  41.2 us (15%)
  starting transfers between devices  28.5 us (10%)
  matrix products  22.3 us (8%)
  between operations  13.6 us (5%)
    all_gather x1, waiting for transfers between devices, on_device(): piece = lax.all_gather(shared, 'tp', axis=1, tiled=True)  43.6 us
    unnamed x3, waiting for transfers between devices  43.4 us
    all_to_all x1, waiting for transfers between devices, on_device(): lax.all_to_all(leaving, 'ep', split_axis=1, concat_axis=1, tiled=True)  23.7 us
    and x1, other arithmetic, on_device(): shared = jnp.take(arrived.reshape(-1, share_width), arrival, axis=0)  16.2 us
    gather x3, local copies, waits for them, and re-layouts, on_device(): jnp.take_along_axis(chosen, send_pos, axis=1) - device * tok_rows  12.8 us
    unnamed x18, local copies, waits for them, and re-layouts  12.3 us
    all_to_all x1, starting transfers between devices, on_device(): lax.all_to_all(outgoing, 'ep', split_axis=0, concat_axis=0, tiled=True)  11.9 us
    dot_general x1, matrix products, on_device(): lax.dot_general(piece, hidden, (((0,), (1,)), ((), ())), preferred_elemen...  11.4 us
  transfers between devices with their start and end apart: 5, of which 5 were waited for; matrix products, arithmetic and copies ran while one was open for 11% of the time, Pallas kernels for 0%

commit v1 on v0

--- a/solution.py
+++ b/solution.py
@@ -56,7 +56,9 @@
     outgoing = jnp.take(own_columns, local_flat, axis=0).reshape(experts, slots, share_width)
     arrived = lax.all_to_all(outgoing, "ep", split_axis=0, concat_axis=0, tiled=True)
     shared = jnp.take(arrived.reshape(-1, share_width), arrival, axis=0)
-    piece = lax.all_gather(shared, "tp", axis=1, tiled=True)
+    piece = jnp.concatenate(
+        lax.all_to_all(jnp.stack([shared] * lax.axis_size("tp")), "tp", 0, 0), axis=1
+    )
     gate = jnp.dot(piece, gate_rows, preferred_element_type=jnp.float32)
     up = jnp.dot(piece, up_rows, preferred_element_type=jnp.float32)
     hidden = (jax.nn.silu(gate) * up).astype(jnp.bfloat16)

time: 275 us -> 307 us (1.12)
  blocking collectives: 0 us -> 78.6 us
  waiting for transfers between devices: 120 us -> 72.9 us
  local copies, waits for them, and re-layouts: 47.3 us -> 52.1 us
  matrix products: 22.3 us -> 19 us
    all_to_all x0 -> x1, blocking collectives: none -> 78.6 us  [on_device(): lax.all_to_all(jnp.stack([shared] * lax.axis_size('tp')), 'tp', 0, 0)]
    all_gather x1 -> x0, waiting for transfers between devices: 43.6 us -> none  [on_device(): piece = lax.all_gather(shared, 'tp', axis=1, tiled=True)]
    unnamed x3 -> x2, waiting for transfers between devices: 43.4 us -> 39.5 us
    dot_general x1, matrix products: 8.03 us -> 4.59 us  [on_device(): gate = jnp.dot(piece, gate_rows, preferred_element_type=jnp.float32)]
    unnamed x18 -> x22, local copies, waits for them, and re-layouts: 12.3 us -> 14.9 us
  transfers between devices with their start and end apart: 5 -> 4, of which waited for: 5 -> 4; matrix products, arithmetic and copies ran while one was open for 11% -> 10% of each run, Pallas kernels for 0% -> 0%
where the time goes in v1:
time: 307 us; the launch traced here: 306 us
  blocking collectives  78.6 us (26%)
  waiting for transfers between devices  72.9 us (24%)
  local copies, waits for them, and re-layouts  52.1 us (17%)
  other arithmetic  41.2 us (13%)
  starting transfers between devices  28.4 us (9%)
  matrix products  19 us (6%)
  between operations  13.6 us (4%)
    all_to_all x1, blocking collectives, on_device(): lax.all_to_all(jnp.stack([shared] * lax.axis_size('tp')), 'tp', 0, 0)  78.6 us
    unnamed x2, waiting for transfers between devices  39.5 us
    all_to_all x1, waiting for transfers between devices, on_device(): lax.all_to_all(leaving, 'ep', split_axis=1, concat_axis=1, tiled=True)  23.7 us
    and x1, other arithmetic, on_device(): shared = jnp.take(arrived.reshape(-1, share_width), arrival, axis=0)  16.2 us
    unnamed x22, local copies, waits for them, and re-layouts  14.9 us
    gather x3, local copies, waits for them, and re-layouts, on_device(): jnp.take_along_axis(chosen, send_pos, axis=1) - device * tok_rows  12.8 us
    all_to_all x1, starting transfers between devices, on_device(): lax.all_to_all(outgoing, 'ep', split_axis=0, concat_axis=0, tiled=True)  11.9 us
    dot_general x1, matrix products, on_device(): lax.dot_general(piece, hidden, (((0,), (1,)), ((), ())), preferred_elemen...  11.5 us
  transfers between devices with their start and end apart: 4, of which 4 were waited for; matrix products, arithmetic and copies ran while one was open for 10% of the time, Pallas kernels for 0%

profile of v1, /device:TPU:1, one launch (start us, length us, event | category | flops | bytes accessed | tf_op | source)
XLA Modules:
  0.0 305.9 jit_solution(17928445083725890768)
XLA Ops:
  6.5 2.0 multiply_reduce_fusion
  8.5 0.1 copy-done.3
  8.6 2.0 convert_element_type.34
  10.6 0.1 lt.201
  10.7 0.1 add_select_fusion
  10.8 0.0 copy-start.5
  10.8 0.6 copy-done.5
  11.5 0.6 convert_reduce_fusion
  12.1 0.2 reduce_window_sum.11
  12.3 0.2 select_reduce_fusion
  12.5 0.1 fusion.21
  12.6 0.1 add.254
  12.7 0.6 copy-done.6
  13.3 0.1 add.280
  13.3 0.1 reshape.542
  13.4 12.6 %gather_fusion.3 = s32[1536]{0:T(1024)S(1)} fusion(s32[32,1024]{1,0:T(8,128)S(1)} %copy-done.1, s32[1536]{0:T(1024)S(1)} %reshape.542), kind=kCustom, calls=%fused_computation.3 | custom fusion | bytes 24576 | tf_op jit(solution)/shard_map/jit(take_along_axis)/gather | solution.py:45
  26.0 0.1 reshape.545
  26.1 0.1 compare_and_fusion
  26.2 0.1 lt.199
  26.3 0.1 fusion.25
  26.4 0.8 dynamic-slice.15
  27.2 1.1 multiply_convert_fusion.3
  28.3 5.3 %gather_fusion = bf16[1536,384]{1,0:T(8,128)(2,1)} fusion(bf16[256,384]{1,0:T(8,128)(2,1)S(1)} %multiply_convert_fusion.3, s32[2048]{0:T(1024)S(1)} %pad_clamp_fusion.1), kind=kCustom, calls=%fused_computation | custom fusion | bytes 2365440 | tf_op jit(solution)/shard_map/jit(_take)/gather | solution.py:56
  33.6 2.6 broadcast_select_fusion
  36.1 11.9 %all-to-all-start = ((bf16[32,48,384]{2,1,0:T(8,128)(2,1)}), bf16[32,48,384]{2,1,0:T(8,128)(2,1)S(1)}, u32[]{:S(2)}, u32[]{:S(2)}) async-start(bf16[32,48,384]{2,1,0:T(8,128)(2,1)} %broadcast_select_fusion), calls=%async_computation | async-start | bytes 2359296 | tf_op jit(solution)/shard_map/all_to_all | solution.py:57
  48.0 0.0 reduce-scatter.4.cloned.1.call-start
  48.0 0.7 broadcast_select_fusion.4
  48.7 0.7 fusion.30
  49.5 4.9 %compare_select_fusion.10 = (s32[1024,1]{0,1:T(1,128)S(1)}, s32[1024,1]{0,1:T(1,128)S(1)}, s32[1,1024]{1,0:T(1,128)S(1)}) fusion(s32[]{:T(128)} %bitcast.28, s32[]{:T(128)} %bitcast.29, s32[]{:T(128)} %bitcast.30, s32[]{:T(128)} %bitcast.31, s32[]{:T(128)} %bitcast.32, s32[]{:T(128)} %bitcast.34, s32[]{:T(128)} %bitcast.33, s32[32,1024]{1,0:T(8,128)} %copy-done.5, ...), kind=kLoop, calls=%fused_computation.80 | loop fusion | flops 16384 | bytes 16417 | tf_op jit(solution)/shard_map/jit(_take)/gather | solution.py:51
  54.4 0.7 fusion.31
  55.1 0.3 compare_reduce_fusion.24
  55.3 16.2 %compare_and_fusion.2 = (pred[1024]{0:T(1024)(128)(4,1)}, s32[1024]{0:T(1024)S(1)}) fusion(s32[1024]{0:T(1024)S(1)} %bitcast.93, pred[1024]{0:T(1024)(128)(4,1)S(1)} %get-tuple-element.63, pred[1024]{0:T(1024)(128)(4,1)S(1)} %get-tuple-element.61, pred[1024]{0:T(1024)(128)(4,1)S(1)} %get-tuple-element.62, pred[1024]{0:T(1024)(128)(4,1)S(1)} %get-tuple-element.60, ...), kind=kLoop, calls=%fused_computation.101 | loop fusion | flops 41984 | bytes 39012 | tf_op jit(solution)/shard_map/jit(_take)/and | solution.py:58
  71.6 5.1 %all-to-all-done = bf16[32,48,384]{2,1,0:T(8,128)(2,1)S(1)} async-done(((bf16[32,48,384]{2,1,0:T(8,128)(2,1)}), bf16[32,48,384]{2,1,0:T(8,128)(2,1)S(1)}, u32[]{:S(2)}, u32[]{:S(2)}) %all-to-all-start) | async-done | bytes 1179680 | tf_op jit(solution)/shard_map/all_to_all | solution.py:57
  76.7 5.0 %gather_fusion.1 = bf16[1024,384]{1,0:T(8,128)(2,1)} fusion(bf16[1536,384]{1,0:T(8,128)(2,1)S(1)} %bitcast.87, s32[1024]{0:T(1024)S(1)} %broadcast_clamp_fusion), kind=kCustom, calls=%fused_computation.1 | custom fusion | bytes 1576960 | tf_op jit(solution)/shard_map/jit(_take)/gather | solution.py:58
  81.6 2.2 broadcast_select_fusion.2
  83.8 1.4 copy.12
  85.3 0.8 stack.2
  86.1 78.6 %all_to_all.21 = bf16[8,1024,384]{1,2,0:T(8,128)(2,1)S(1)} all-to-all(bf16[8,1024,384]{1,2,0:T(8,128)(2,1)S(1)} %stack.2), channel_id=1, replica_groups=mesh['ep'=32,'tp'=8] {'tp'}, dimensions={0} | all-to-all | bytes 12582912 | tf_op jit(solution)/shard_map/all_to_all | solution.py:60
  164.7 2.7 copy-done.2
  167.3 4.6 %fusion.3 = f32[1024,384]{1,0:T(8,128)} fusion(bf16[1024,3072]{0,1:T(8,128)(2,1)S(1)} %bitcast.88, bf16[1,3072,384]{2,1,0:T(8,128)(2,1)S(1)} %copy-done.4), kind=kOutput, calls=%fused_computation.11 | convolution fusion | flops 2415919104 | bytes 10223616 | tf_op jit(solution)/shard_map/dot_general | solution.py:62
  171.9 11.5 %convert_bitcast_fusion = bf16[3072,1024]{0,1:T(8,128)(2,1)} fusion(bf16[1,384,3072]{2,1,0:T(8,128)(2,1)S(1)} %copy-done, f32[1024,384]{1,0:T(8,128)} %fusion.3, bf16[1024,3072]{0,1:T(8,128)(2,1)} %bitcast.89, bf16[1,3072,384]{2,1,0:T(8,128)(2,1)} %param.15), kind=kOutput, calls=%fused_computation.4 | convolution fusion | flops 4837343232 | bytes 18874368 | tf_op jit(solution)/shard_map/dot_general | solution.py:68
  183.5 8.6 %copy.14 = bf16[3072,1024]{1,0:T(8,128)(2,1)} copy(bf16[3072,1024]{0,1:T(8,128)(2,1)} %convert_bitcast_fusion) | data formatting | bytes 12582912
  192.1 0.0 reduce-scatter.4.cloned.1.call-update
  192.1 0.7 fusion.35
  192.8 0.1 add_clamp_fusion
  192.9 0.1 min.35
  193.0 0.1 compare_and_fusion.1
  193.1 39.5 %reduce-scatter.4.cloned.1.call-done = bf16[384,1024]{1,0:T(8,128)(2,1)} async-done(((bf16[3072,1024]{1,0:T(8,128)(2,1)}), bf16[384,1024]{1,0:T(8,128)(2,1)}) %reduce-scatter.4.cloned.1.call-update) | async-done | bytes 786448
  232.6 2.3 copy.15
  234.9 1.3 multiply_convert_fusion
  236.3 5.3 %gather_fusion.2 = bf16[1536,384]{1,0:T(8,128)(2,1)} fusion(bf16[384,1024]{0,1:T(8,128)(2,1)S(1)} %multiply_convert_fusion, s32[2048]{0:T(1024)S(1)} %pad_clamp_fusion), kind=kCustom, calls=%fused_computation.2 | custom fusion | bytes 2365440 | tf_op jit(solution)/shard_map/jit(_take)/gather | solution.py:77
  241.6 2.6 broadcast_select_fusion.1
  244.1 9.5 %all-to-all-start.2 = ((bf16[384,32,48]{0,2,1:T(8,128)(2,1)}), bf16[384,32,48]{0,2,1:T(8,128)(2,1)S(1)}, u32[]{:S(2)}, u32[]{:S(2)}) async-start(bf16[384,32,48]{0,2,1:T(8,128)(2,1)} %broadcast_select_fusion.1), calls=%async_computation.2 | async-start | bytes 2359296 | tf_op jit(solution)/shard_map/all_to_all | solution.py:78
  253.7 1.4 add.255
  255.0 0.7 lt.182
  255.7 0.6 lt.183
  256.3 0.8 lt.184
  257.1 1.3 subtract_select_fusion
  258.4 23.7 %all-to-all-done.2 = bf16[384,32,48]{0,2,1:T(8,128)(2,1)S(1)} async-done(((bf16[384,32,48]{0,2,1:T(8,128)(2,1)}), bf16[384,32,48]{0,2,1:T(8,128)(2,1)S(1)}, u32[]{:S(2)}, u32[]{:S(2)}) %all-to-all-start.2) | async-done | bytes 1179680 | tf_op jit(solution)/shard_map/all_to_all | solution.py:78
  282.1 2.9 multiply_reduce_fusion.1
  285.0 0.6 broadcast_in_dim.111
  285.6 7.0 %all-to-all-start.3 = ((f32[8,1,256]{2,1,0:T(1,128)}), f32[8,1,256]{2,1,0:T(1,128)S(1)}, u32[]{:S(2)}, u32[]{:S(2)}) async-start(f32[8,1,256]{2,1,0:T(1,128)} %broadcast_in_dim.111), calls=%async_computation.3 | async-start | bytes 16384 | tf_op jit(solution)/shard_map/all_to_all | solution.py:11
  292.6 4.6 %all-to-all-done.3 = f32[8,1,256]{2,1,0:T(1,128)S(1)} async-done(((f32[8,1,256]{2,1,0:T(1,128)}), f32[8,1,256]{2,1,0:T(1,128)S(1)}, u32[]{:S(2)}, u32[]{:S(2)}) %all-to-all-start.3) | async-done | bytes 8224 | tf_op jit(solution)/shard_map/all_to_all | solution.py:11
  297.3 1.8 multiply_convert_fusion.2
  (26 shorter events, 0.1 us)
Async XLA Ops:
  6.5 165.4 %copy-start = (bf16[1,384,3072]{2,1,0:T(8,128)(2,1)S(1)}, bf16[1,384,3072]{2,1,0:T(8,128)(2,1)}, u32[]{:S(2)}) copy-start(bf16[1,384,3072]{2,1,0:T(8,128)(2,1)} %param.16) | copy-start | bytes 7077892
  6.5 2.0 copy-start.3
  8.6 2.1 copy-start.1
  10.8 0.7 copy-start.5
  12.3 13.7 %copy-start.7 = (s32[32,32]{1,0:T(8,128)}, s32[32,32]{1,0:T(8,128)S(1)}, u32[]{:S(2)}) copy-start(s32[32,32]{1,0:T(8,128)S(1)} %sub.52) | copy-start | bytes 12292
  12.7 0.6 copy-start.6
  36.1 40.5 %all-to-all-start = ((bf16[32,48,384]{2,1,0:T(8,128)(2,1)}), bf16[32,48,384]{2,1,0:T(8,128)(2,1)S(1)}, u32[]{:S(2)}, u32[]{:S(2)}) async-start(bf16[32,48,384]{2,1,0:T(8,128)(2,1)} %broadcast_select_fusion), calls=%async_computation | async-start | bytes 2359296 | tf_op jit(solution)/shard_map/all_to_all | solution.py:57
  48.0 184.6 %reduce-scatter.4.cloned.1.call-start = ((), (), s32[]{:S(2)}) async-start(), calls=%async_computation.5 | async-start | bytes 7077888
  86.1 81.3 %copy-start.4 = (bf16[1,3072,384]{2,1,0:T(8,128)(2,1)S(1)}, bf16[1,3072,384]{2,1,0:T(8,128)(2,1)}, u32[]{:S(2)}) copy-start(bf16[1,3072,384]{2,1,0:T(8,128)(2,1)} %param.14) | copy-start | bytes 7077892
  164.7 2.7 copy-start.2
  192.1 42.8 %copy-start.8 = (f32[1,1024]{1,0:T(1,128)S(1)}, f32[1,1024]{1,0:T(1,128)}, u32[]{:S(2)}) copy-start(f32[1,1024]{1,0:T(1,128)} %param.13) | copy-start | bytes 12292
  244.1 38.0 %all-to-all-start.2 = ((bf16[384,32,48]{0,2,1:T(8,128)(2,1)}), bf16[384,32,48]{0,2,1:T(8,128)(2,1)S(1)}, u32[]{:S(2)}, u32[]{:S(2)}) async-start(bf16[384,32,48]{0,2,1:T(8,128)(2,1)} %broadcast_select_fusion.1), calls=%async_computation.2 | async-start | bytes 2359296 | tf_op jit(solution)/shard_map/all_to_all | solution.py:78
  258.4 34.2 %copy-start.9 = (bf16[384]{0:T(512)(128)(2,1)S(1)}, bf16[384]{0:T(512)(128)(2,1)}, u32[]{:S(2)}) copy-start(bf16[384]{0:T(512)(128)(2,1)} %param.17) | copy-start | bytes 2308
  285.6 11.6 %all-to-all-start.3 = ((f32[8,1,256]{2,1,0:T(1,128)}), f32[8,1,256]{2,1,0:T(1,128)S(1)}, u32[]{:S(2)}, u32[]{:S(2)}) async-start(f32[8,1,256]{2,1,0:T(1,128)} %broadcast_in_dim.111), calls=%async_computation.3 | async-start | bytes 16384 | tf_op jit(solution)/shard_map/all_to_all | solution.py:11
Sparse Core Ops, SparseCore 0:
  192.2 40.3 reduce-scatter.3
